TPU v7x, 32 devices: a whole 2x2x4 slice. The times are simulated.
32 devices in a mesh: sp: 8 (over z, x), tp: 4 (over y, core).
Axes of the slice: x: 2, y: 2, z: 4, core: 2. Of those that a mesh axis runs over, the one named last changes fastest.
Arguments:
- tokens: bfloat16 [1024, 1024], P(('sp', 'tp')), may hold values from -13 to 13, as said below
- norm_gain: float32 [1024], replicated, may hold values from 0.5 to 1.5
- query_weight: bfloat16 [1024, 4096], P(None, 'tp'), may hold values from -0.1875 to 0.1875
- key_weight: bfloat16 [1024, 512], P(None, 'tp'), may hold values from -0.1875 to 0.1875
- value_weight: bfloat16 [1024, 512], P(None, 'tp'), may hold values from -0.1875 to 0.1875
- query_gain: float32 [128], replicated, may hold values from 0.5 to 1.5
- key_gain: float32 [128], replicated, may hold values from 0.5 to 1.5
- output_weight: bfloat16 [4096, 1024], P('tp'), may hold values from -0.25 to 0.25
Outputs:
- mixed: bfloat16 [1024, 1024], P(('sp', 'tp'))
Inputs may be any that keep to these rules, and one draw needn't show every extreme that they name: Every entry of tokens lies between -13 and 13.
All inputs are finite; a program needn't handle non-finite values.
Results may differ from a plain program's by a relative error of at most 0.015.
Values may be sent and summed in bfloat16 or wider, within the bound.
A program may use at most 64 MiB of HBM per device.

v0:
```python
import math

import jax
import jax.numpy as jnp
from jax import lax
from jax.sharding import PartitionSpec as P

GRID_W = 64


epsilon = 1e-06
rotary_base = 10000.0


def gathered_then(array, axis, dim, block):
    whole = lax.all_gather(array, axis, axis=dim, tiled=True)
    return block(whole, jnp.int32(0))


def folded_2(shard, axis, dim, absorb, state):
    everything = jax.tree.map(lambda a: lax.all_gather(a, axis, axis=dim, tiled=True), shard)
    return absorb(state, everything, jnp.int32(0))


def summed_rows(product, span, axis):
    everything = product(jnp.int32(0), lax.axis_size(axis) * span)
    own = lax.psum_scatter(everything.astype(jnp.bfloat16), axis, scatter_dimension=0, tiled=True)
    return own.astype(jnp.float32)


def rotation_tables(first_position, length, head_dim):
    positions = first_position + lax.iota(jnp.int32, length)
    grid_row = (positions // GRID_W).astype(jnp.float32)
    grid_column = (positions % GRID_W).astype(jnp.float32)
    axis_dim = head_dim // 2
    frequencies = rotary_base ** (-jnp.arange(0, axis_dim, 2, dtype=jnp.float32) / axis_dim)
    angles = jnp.concatenate(
        [grid_row[:, None] * frequencies[None, :], grid_column[:, None] * frequencies[None, :]],
        axis=-1,
    )
    return (jnp.cos(angles), jnp.sin(angles))


def normalize_rotate(projected, gain, cosine, sine):
    widened = projected.astype(jnp.float32)
    scaled = (
        widened
        * lax.rsqrt(jnp.mean(widened * widened, axis=-1, keepdims=True) + epsilon)
        * gain.astype(jnp.float32)
    )
    paired = scaled.reshape(scaled.shape[:-1] + (scaled.shape[-1] // 2, 2))
    even_half = paired[..., 0]
    odd_half = paired[..., 1]
    cosine_rows = cosine[:, None, :]
    sine_rows = sine[:, None, :]
    turned = jnp.stack(
        [
            even_half * cosine_rows - odd_half * sine_rows,
            even_half * sine_rows + odd_half * cosine_rows,
        ],
        axis=-1,
    )
    return turned.reshape(projected.shape).astype(jnp.bfloat16)


def rms_rows(tokens, norm_gain):
    widened = tokens.astype(jnp.float32)
    scaled = widened * lax.rsqrt(jnp.mean(widened * widened, axis=-1, keepdims=True) + epsilon)
    return (scaled * norm_gain.astype(jnp.float32)).astype(jnp.bfloat16)


def per_device(
    tokens, norm_gain, query_weight, key_weight, value_weight, query_gain, key_gain, output_weight
):
    head_dim = query_gain.shape[0]
    query_width = query_weight.shape[1]
    group_width = key_weight.shape[1]
    query_heads = query_width // head_dim
    group_heads = group_width // head_dim
    group_size = query_heads // group_heads
    normed = rms_rows(tokens, norm_gain)

    def project(piece, start):
        query_part = jnp.dot(piece, query_weight, preferred_element_type=jnp.float32).astype(
            jnp.bfloat16
        )
        key_part = jnp.dot(piece, key_weight, preferred_element_type=jnp.float32).astype(
            jnp.bfloat16
        )
        value_part = jnp.dot(piece, value_weight, preferred_element_type=jnp.float32).astype(
            jnp.bfloat16
        )
        return jnp.concatenate([query_part, key_part, value_part], axis=1)

    projected = gathered_then(normed, "tp", 0, project)
    block_len = projected.shape[0]
    cosine, sine = rotation_tables(lax.axis_index("sp") * block_len, block_len, head_dim)
    queries = normalize_rotate(
        projected[:, :query_width].reshape(block_len, query_heads, head_dim),
        query_gain,
        cosine,
        sine,
    )
    keys = normalize_rotate(
        projected[:, query_width : query_width + group_width].reshape(
            block_len, group_heads, head_dim
        ),
        key_gain,
        cosine,
        sine,
    )
    values = projected[:, query_width + group_width :].reshape(block_len, group_heads, head_dim)
    query_rows = group_size * block_len
    grouped = queries.reshape(block_len, group_heads, group_size, head_dim).transpose(1, 2, 0, 3)
    grouped = grouped.reshape(group_heads, query_rows, head_dim)
    scale = head_dim ** (-0.5)

    def block_scores(key_block):
        return (
            jnp.einsum("kqd,skd->kqs", grouped, key_block, preferred_element_type=jnp.float32)
            * scale
        )

    def weighted_values(weights, value_block):
        return jnp.einsum(
            "kqs,skd->kqd",
            weights.astype(jnp.bfloat16),
            value_block,
            preferred_element_type=jnp.float32,
        )

    zero_sums = jnp.zeros((group_heads, query_rows), jnp.float32)
    zero_values = jnp.zeros((group_heads, query_rows, head_dim), jnp.float32)
    ceiling = 1.02 * math.sqrt(head_dim) * jnp.max(jnp.abs(query_gain)) * jnp.max(jnp.abs(key_gain))

    def fold_step(carry, blocks):
        denominator, numerator = carry
        weights = jnp.exp(block_scores(blocks[0]) - ceiling)
        denominator = denominator + jnp.sum(weights, axis=-1)
        numerator = numerator + weighted_values(weights, blocks[1])
        return ((denominator, numerator), None)

    initial = (zero_sums, zero_values)

    def fold_keys(carry, pieces, start):
        block_count = pieces[0].shape[0] // block_len
        key_blocks = pieces[0].reshape(block_count, block_len, group_heads, head_dim)
        value_blocks = pieces[1].reshape(block_count, block_len, group_heads, head_dim)
        carry, unused = lax.scan(fold_step, carry, (key_blocks, value_blocks))
        return carry

    folded = folded_2((keys, values), "sp", 0, fold_keys, initial)
    attended = (folded[-1] / folded[-2][..., None]).astype(jnp.bfloat16)
    attended = attended.reshape(group_heads, group_size, block_len, head_dim).transpose(2, 0, 1, 3)
    attended = attended.reshape(block_len, query_width)

    def head_sum(start, count):
        rows_taken = lax.dynamic_slice_in_dim(attended, start, count, 0)
        return jnp.dot(rows_taken, output_weight, preferred_element_type=jnp.float32)

    mixed = summed_rows(head_sum, tokens.shape[0], "tp")
    return mixed.astype(jnp.bfloat16)


def solution(mesh):
    return jax.shard_map(
        per_device,
        mesh=mesh,
        in_specs=(
            P(("sp", "tp"), None),
            P(),
            P(None, "tp"),
            P(None, "tp"),
            P(None, "tp"),
            P(),
            P(),
            P("tp", None),
        ),
        out_specs=P(("sp", "tp"), None),
        check_vma=False,
    )
```

profile of v0, /device:TPU:0, one launch (start us, length us, event | category | flops | bytes accessed | tf_op | source)
XLA Modules:
  0.0 135.4 jit_solution(16290751525785200599)
XLA Ops:
  6.5 0.0 copy-start
  6.5 0.0 reduce-scatter.2.cloned.1.call-start
  6.6 1.1 fusion.14
  7.7 0.9 fusion.16
  8.6 7.3 %all_gather.9 = bf16[128,1024]{1,0:T(8,128)(2,1)S(1)} all-gather(bf16[32,1024]{1,0:T(8,128)(2,1)S(1)} %fusion.16), channel_id=1, replica_groups=mesh['sp'=8,'tp'=4] {'tp'}, dimensions={0}, use_global_device_ids=true | all-gather | bytes 327680 | tf_op jit(solution)/shard_map/all_gather | solution.py:16
  15.9 0.0 copy-done
  15.9 0.0 copy-start.2
  15.9 0.4 fusion.12
  16.3 0.8 multiply_bitcast_fusion
  17.2 0.2 copy.52
  17.4 0.0 copy-done.2
  17.4 0.1 mul.222
  17.5 0.7 abs_reduce_fusion.1
  18.2 1.9 %copy.62 = f32[16,8,8,128]{3,2,1,0:T(8,128)} copy(f32[16,8,8,128]{3,1,2,0:T(8,128)} %multiply_bitcast_fusion) | data formatting | bytes 1048576
  20.2 1.2 reduce_sum.40
  21.5 0.1 broadcast_multiply_fusion.1
  21.6 0.2 fusion.18
  21.7 0.0 copy-start.3
  21.7 0.3 multiply_multiply_fusion
  22.0 0.7 subtract_convert_fusion
  22.7 0.0 copy-start.1
  22.7 0.6 pad_maximum_fusion
  23.3 0.3 copy.54
  23.6 0.9 copy.59
  24.5 1.2 multiply_reduce_fusion
  25.8 0.0 copy-done.3
  25.8 0.7 abs_reduce_fusion
  26.5 0.1 multiply_multiply_fusion.1
  26.6 0.1 fusion.26
  26.6 0.1 subtract_convert_fusion.1
  26.8 31.3 %all_gather.10 = bf16[1024,1,128]{0,2,1:T(8,128)(2,1)S(1)} all-gather(bf16[128,1,128]{0,2,1:T(8,128)(2,1)S(1)} %bitcast.76), channel_id=1, replica_groups=mesh['sp'=8,'tp'=4] {'sp'}, dimensions={0}, use_global_device_ids=true | all-gather | bytes 294912 | tf_op jit(solution)/shard_map/all_gather | solution.py:21
  58.1 0.8 copy.51
  59.0 0.0 copy-done.1
  59.0 0.2 convolution_convert_fusion.2
  59.2 30.7 %all-gather = bf16[1024,128]{1,0:T(8,128)(2,1)S(1)} all-gather(bf16[128,128]{1,0:T(8,128)(2,1)S(1)} %convolution_convert_fusion.2), channel_id=2, replica_groups=mesh['sp'=8,'tp'=4] {'sp'}, dimensions={0}, use_global_device_ids=true | all-gather | bytes 294912 | tf_op jit(solution)/shard_map/all_gather | solution.py:21
  91.3 12.9 %while.13 = (s32[]{:T(128)}, f32[1,1024]{1,0:T(1,128)S(1)}, f32[1,1024,128]{2,1,0:T(8,128)S(1)}, bf16[8,128,1,128]{3,1,2,0:T(8,128)(2,1)}, bf16[1,1024,128]{2,1,...) while((s32[]{:T(128)}, f32[1,1024]{1,0:T(1,128)S(1)}, ...), condition=%wide.region_7.8_spmd.clone, body=%wide.region_5.7_spmd.clone.sunk | while | flops 67896320 | bytes 1918060 | solution.py:149
  91.3 1.2 fusion.43
  92.6 0.3 fusion.45
  92.9 1.2 fusion.43
  94.2 0.3 fusion.45
  94.5 1.2 fusion.43
  95.8 0.3 fusion.45
  96.1 1.3 fusion.43
  97.4 0.3 fusion.45
  97.8 1.3 fusion.43
  99.0 0.3 fusion.45
  99.4 1.2 fusion.43
  100.6 0.3 fusion.45
  101.0 1.2 fusion.43
  102.2 0.3 fusion.45
  102.6 1.2 fusion.43
  103.8 0.3 fusion.45
  104.2 0.2 divide_convert_fusion
  104.4 0.2 copy.58
  104.6 2.8 %convolution_convert_fusion = bf16[128,1024]{1,0:T(8,128)(2,1)} fusion(bf16[128,1024]{0,1:T(8,128)(2,1)S(1)} %bitcast.69, bf16[1024,1024]{1,0:T(8,128)(2,1)} %param.17), kind=kOutput, calls=%fused_computation.15 | convolution fusion | flops 268566528 | bytes 2621440 | tf_op jit(solution)/shard_map/dot_general | solution.py:159
  107.3 0.0 reduce-scatter.2.cloned.1.call-update
  107.4 21.2 %reduce-scatter.2.cloned.1.call-done = bf16[32,1024]{1,0:T(8,128)(2,1)} async-done(((bf16[128,1024]{1,0:T(8,128)(2,1)}), bf16[32,1024]{1,0:T(8,128)(2,1)}) %reduce-scatter.2.cloned.1.call-update) | async-done | bytes 65552 | tf_op jit(solution)/shard_map/reduce_scatter | solution.py:27
  (18 shorter events, 0.3 us)
Async XLA Ops:
  6.5 9.4 %copy-start = (bf16[1024,1024]{1,0:T(8,128)(2,1)S(1)}, bf16[1024,1024]{1,0:T(8,128)(2,1)}, u32[]{:S(2)}) copy-start(bf16[1024,1024]{1,0:T(8,128)(2,1)} %param.12) | copy-start | bytes 6291460
  6.5 122.1 %reduce-scatter.2.cloned.1.call-start = ((), (), s32[]{:S(2)}) async-start(), calls=%async_computation.1 | async-start | bytes 327680 | tf_op jit(solution)/shard_map/reduce_scatter | solution.py:27
  15.9 1.5 %copy-start.2 = (f32[128]{0:T(128)S(1)}, f32[128]{0:T(128)}, u32[]{:S(2)}) copy-start(f32[128]{0:T(128)} %param.15) | copy-start | bytes 1540
  21.7 4.0 %copy-start.3 = (f32[128]{0:T(128)S(1)}, f32[128]{0:T(128)}, u32[]{:S(2)}) copy-start(f32[128]{0:T(128)} %param.16) | copy-start | bytes 1540
  22.7 36.3 %copy-start.1 = (bf16[1024,128]{1,0:T(8,128)(2,1)S(1)}, bf16[1024,128]{1,0:T(8,128)(2,1)}, u32[]{:S(2)}) copy-start(bf16[1024,128]{1,0:T(8,128)(2,1)} %param.14) | copy-start | bytes 786436
Sparse Core Ops, SparseCore 0:
  107.5 21.0 reduce-scatter.1
where the time goes:
time: 136 us; the launch traced here: 135 us
  blocking collectives  69.3 us (51%)
  waiting for transfers between devices  21.2 us (16%)
  matrix products  17.1 us (13%)
  between operations  15 us (11%)
  other arithmetic  7.86 us (6%)
  local copies, waits for them, and re-layouts  4.64 us (3%)
    all_gather x2, blocking collectives, folded_2(): lax.all_gather(a, axis, axis=dim, tiled=True)  62 us
    reduce_scatter x1, waiting for transfers between devices, summed_rows(): lax.psum_scatter(everything.astype(jnp.bfloat16), axis, scatter_dimension...  21.2 us
    dot_general x8, matrix products, block_scores(): jnp.einsum('kqd,skd->kqs', grouped, key_block, preferred_element_type=jnp...  9.99 us
    all_gather x1, blocking collectives, gathered_then(): whole = lax.all_gather(array, axis, axis=dim, tiled=True)  7.28 us
    unnamed x10, local copies, waits for them, and re-layouts  2.86 us
    dot_general x1, matrix products, head_sum(): jnp.dot(rows_taken, output_weight, preferred_element_type=jnp.float32)  2.77 us
  transfers between devices with their start and end apart: 1, of which 1 were waited for; matrix products, arithmetic and copies ran while one was open for 0% of the time, Pallas kernels for 0%

commit v1 on v0

v1 whole, which is shorter than its diff:
```python
import functools
import math

import jax
import jax.numpy as jnp
import numpy as np
from jax import lax
from jax.experimental import pallas as pl
from jax.experimental.pallas import tpu as pltpu

from jax.sharding import PartitionSpec as P

GRID_W = 64
EPS = 1e-06
ROTARY_BASE = 10000.0
MESH = pl.DeviceIdType.MESH
F32 = jnp.float32
BF16 = jnp.bfloat16
UNROLL = 8


def angle_tables(grid_rows, head_dim):
    half = head_dim // 2
    freq = np.float32(ROTARY_BASE) ** (-np.arange(0, half, 2, dtype=np.float32) / np.float32(half))
    freq = np.repeat(freq.astype(np.float32), 2)
    sign = np.tile(np.array([-1.0, 1.0], np.float32), half // 2)
    zero = lambda n: np.zeros((n, half), np.float32)
    row = np.arange(grid_rows, dtype=np.float32)[:, None] * freq[None, :]
    col = np.arange(GRID_W, dtype=np.float32)[:, None] * freq[None, :]
    rows = np.stack(
        [
            np.concatenate([np.cos(row), zero(grid_rows)], 1),
            np.concatenate([np.sin(row) * sign, zero(grid_rows)], 1),
        ]
    )
    cols = np.stack(
        [
            np.concatenate([zero(GRID_W), np.cos(col)], 1),
            np.concatenate([zero(GRID_W), np.sin(col) * sign], 1),
        ]
    )
    return rows.astype(np.float32), cols.astype(np.float32)


def repeat(start, stop, body):
    if stop - start <= UNROLL:
        for i in range(start, stop):
            body(i)
    else:
        lax.fori_loop(start, stop, lambda i, c: (body(i), c)[1], 0)


class PairExchange:
    def __init__(self, axis, n, buf, send, recv):
        self.axis, self.n, self.buf, self.send, self.recv = axis, n, buf, send, recv
        self.half = n // 2
        self.me = lax.axis_index(axis)
        self.partner = self.me + 1 - 2 * (self.me % 2)

    def hop(self, i):
        if isinstance(i, int):
            return (i + 1) // 2 if i % 2 == 1 else self.half - i // 2
        return (i % 2) * ((i + 1) // 2) + (1 - i % 2) * (self.half - i // 2)

    def source(self, i):
        return lax.rem(self.me + self.n - 2 * self.hop(i), self.n)

    def pair_of(self, slot):
        return slot + 1 - 2 * (slot % 2)

    def copy(self, slot, sem, target):
        return pltpu.make_async_remote_copy(
            src_ref=self.buf.at[slot],
            dst_ref=self.buf.at[slot],
            send_sem=self.send.at[sem],
            recv_sem=self.recv.at[slot],
            device_id={self.axis: target},
            device_id_type=MESH,
        )

    def greet(self, barrier):
        pl.semaphore_signal(barrier, inc=1, device_id={self.axis: self.partner}, device_id_type=MESH)

        def one(i):
            target = lax.rem(self.me + 2 * i, self.n)
            pl.semaphore_signal(barrier, inc=1, device_id={self.axis: target}, device_id_type=MESH)

        repeat(1, self.half, one)
        return self.half

    def start(self):
        def one(i):
            self.copy(self.me, i, lax.rem(self.me + 2 * self.hop(i), self.n)).start()

        self.copy(self.me, 0, self.partner).start()
        repeat(1, self.half, one)

    def forward(self, i):
        slot = self.source(i)
        self.copy(slot, 0, self.partner).wait_recv()
        self.copy(slot, self.half + i, self.partner).start()

    def wait_slot(self, slot):
        self.copy(slot, 0, self.partner).wait_recv()

    def finish(self):
        def one(i):
            self.copy(self.me, i, self.partner).wait_send()

        def two(i):
            self.copy(self.me, self.half + i, self.partner).wait_send()

        repeat(0, self.half, one)
        repeat(1, self.half, two)


def layer_kernel(
    n_sp,
    n_tp,
    tokens,
    norm_gain,
    wq_hbm,
    wk_hbm,
    wv_hbm,
    query_gain,
    key_gain,
    wo_hbm,
    row_hbm,
    col_hbm,
    out,
    tok,
    gain,
    qgain,
    kgain,
    wq,
    wkv,
    wo,
    rowtab,
    coltab,
    normed,
    kv,
    q,
    num,
    den,
    att,
    own,
    part,
    got,
    lsem,
    tok_send,
    tok_recv,
    kv_send,
    kv_recv,
    rs_send,
    rs_recv,
):
    tp = lax.axis_index("tp")
    sp = lax.axis_index("sp")
    rows, width = tok.shape[1], tok.shape[2]
    block = n_tp * rows
    hd = q.shape[1]
    heads = wq.shape[1] // hd
    tokx = PairExchange("tp", n_tp, tok, tok_send, tok_recv)
    kvx = PairExchange("sp", n_sp, kv, kv_send, kv_recv)

    local = [
        (tokens, tok.at[tp]),
        (norm_gain, gain),
        (wk_hbm, wkv.at[:, pl.ds(0, hd)]),
        (wv_hbm, wkv.at[:, pl.ds(hd, hd)]),
        (key_gain, kgain),
        (query_gain, qgain),
        (row_hbm, rowtab),
        (col_hbm, coltab),
        (wq_hbm, wq),
        (wo_hbm, wo),
    ]
    copies = [pltpu.make_async_copy(a, b, lsem.at[i]) for i, (a, b) in enumerate(local)]
    barrier = pltpu.get_barrier_semaphore()
    copies[0].start()
    count = kvx.greet(barrier) + n_tp - 1
    for k in range(1, n_tp):
        target = lax.rem(tp + k, n_tp)
        pl.semaphore_signal(barrier, inc=1, device_id={"tp": target}, device_id_type=MESH)
    for c in copies[1:]:
        c.start()
    copies[0].wait()
    pl.semaphore_wait(barrier, count)

    tokx.start()

    for c in copies[1:8]:
        c.wait()
    grid_rows = block // GRID_W
    cosine, sine = [], []
    for g in range(grid_rows):
        r = sp * grid_rows + g
        cosine.append(coltab[0] + rowtab[0, pl.ds(r, 1), :])
        sine.append(coltab[1] + rowtab[1, pl.ds(r, 1), :])
    cosine = jnp.concatenate(cosine, 0)
    sine = jnp.concatenate(sine, 0)
    even = lax.broadcasted_iota(jnp.int32, (block, hd), 1) % 2 == 0

    def rotate(projected, head_gain):
        x = projected.astype(BF16).astype(F32)
        x = x * lax.rsqrt(jnp.mean(x * x, axis=-1, keepdims=True) + EPS) * head_gain
        swapped = jnp.where(even, pltpu.roll(x, hd - 1, 1), pltpu.roll(x, 1, 1))
        return (x * cosine + swapped * sine).astype(BF16)

    def norm(slot):
        x = tok[slot].astype(F32)
        x = x * lax.rsqrt(jnp.mean(x * x, axis=-1, keepdims=True) + EPS) * gain[...]
        start = pl.multiple_of(slot * rows, rows)
        normed[pl.ds(start, rows), :] = x.astype(BF16)

    norm(tp)
    for i in range(1, tokx.half):
        tokx.forward(i)
    for i in range(1, tokx.half):
        norm(tokx.source(i))
    tokx.wait_slot(tokx.partner)
    norm(tokx.partner)
    for i in range(1, tokx.half):
        slot = tokx.pair_of(tokx.source(i))
        tokx.wait_slot(slot)
        norm(slot)

    kvp = jnp.dot(normed[...], wkv[...], preferred_element_type=F32)
    kv[sp, 1] = kvp[:, hd:].astype(BF16)
    kv[sp, 0] = rotate(kvp[:, :hd], kgain[...])
    kvx.start()

    copies[8].wait()
    step = 2 * hd
    for c in range(wq.shape[1] // step):
        qp = jnp.dot(normed[...], wq[:, c * step : (c + 1) * step], preferred_element_type=F32)
        for h in range(2):
            base = (2 * c + h) * block
            q[base : base + block, :] = rotate(qp[:, h * hd : (h + 1) * hd], qgain[...])

    factor = hd**-0.5 * math.log2(math.e)

    def fold(slot, first):
        low = slot - slot % 2
        keys = kv[pl.ds(low, 2), 0].reshape(2 * block, hd)
        values = kv[pl.ds(low, 2), 1].reshape(2 * block, hd)
        for h in range(heads):
            span = slice(h * block, (h + 1) * block)
            s = lax.dot_general(
                q[span, :], keys, (((1,), (1,)), ((), ())), preferred_element_type=F32
            )
            w = jnp.exp2(s * factor)
            d = w[:, :hd]
            for j in range(1, 2 * block // hd):
                d = d + w[:, j * hd : (j + 1) * hd]
            v = jnp.dot(w.astype(BF16), values, preferred_element_type=F32)
            if first:
                den[span, :] = d
                num[span, :] = v
            else:
                den[span, :] += d
                num[span, :] += v

    kvx.forward(1)
    kvx.wait_slot(kvx.partner)
    fold(sp, True)

    def middle(i):
        kvx.forward(i)
        slot = kvx.source(i - 1)
        kvx.wait_slot(kvx.pair_of(slot))
        fold(slot, False)

    repeat(2, kvx.half, middle)
    slot = kvx.source(kvx.half - 1)
    kvx.wait_slot(kvx.pair_of(slot))
    fold(slot, False)

    for h in range(heads):
        span = slice(h * block, (h + 1) * block)
        total = jnp.sum(den[span, :], axis=-1, keepdims=True)
        att[:, h * hd : (h + 1) * hd] = (num[span, :] / total).astype(BF16)

    copies[9].wait()
    chunks, chunk = part.shape[0], part.shape[3]

    def share(c, k):
        target = lax.rem(tp + k, n_tp)
        return pltpu.make_async_remote_copy(
            src_ref=part.at[c, target],
            dst_ref=got.at[c, k - 1],
            send_sem=rs_send.at[c, k - 1],
            recv_sem=rs_recv.at[c, k - 1],
            device_id={"tp": target},
            device_id_type=MESH,
        )

    order = [n_tp // 2] + [k for k in range(1, n_tp) if k != n_tp // 2]
    for c in range(chunks):
        p = jnp.dot(att[...], wo[:, c * chunk : (c + 1) * chunk], preferred_element_type=F32)
        own[c] = p.reshape(n_tp, rows, chunk)
        part[c] = p.astype(BF16).reshape(n_tp, rows, chunk)
        for k in order:
            share(c, k).start()
    for c in range(chunks):
        total = own[c, tp]
        for k in order:
            share(c, k).wait_recv()
            total = total + got[c, k - 1].astype(F32)
        out[:, c * chunk : (c + 1) * chunk] = total.astype(BF16)

    for c in range(chunks):
        for k in order:
            share(c, k).wait_send()
    tokx.finish()
    kvx.finish()


def solution(mesh):
    n_sp, n_tp = mesh.shape["sp"], mesh.shape["tp"]

    def per_device(tokens, norm_gain, wq, wk, wv, query_gain, key_gain, wo):
        rows, width = tokens.shape
        hd = query_gain.shape[0]
        block = rows * n_tp
        heads = wq.shape[1] // hd
        out_width = wo.shape[1]
        chunks = 4
        chunk = out_width // chunks
        row_np, col_np = angle_tables(block * n_sp // GRID_W, hd)
        vmem = pltpu.VMEM
        dma = pltpu.SemaphoreType.DMA
        any_spec = pl.BlockSpec(memory_space=pl.ANY)
        return pl.pallas_call(
            functools.partial(layer_kernel, n_sp, n_tp),
            out_shape=jax.ShapeDtypeStruct((rows, out_width), BF16),
            in_specs=[any_spec] * 10,
            out_specs=pl.BlockSpec(memory_space=pltpu.VMEM),
            scratch_shapes=[
                vmem((n_tp, rows, width), BF16),
                vmem((1, width), F32),
                vmem((1, hd), F32),
                vmem((1, hd), F32),
                vmem(wq.shape, BF16),
                vmem((width, 2 * hd), BF16),
                vmem(wo.shape, BF16),
                vmem(row_np.shape, F32),
                vmem(col_np.shape, F32),
                vmem((block, width), BF16),
                vmem((n_sp, 2, block, hd), BF16),
                vmem((heads * block, hd), BF16),
                vmem((heads * block, hd), F32),
                vmem((heads * block, hd), F32),
                vmem((block, heads * hd), BF16),
                vmem((chunks, n_tp, rows, chunk), F32),
                vmem((chunks, n_tp, rows, chunk), BF16),
                vmem((chunks, n_tp - 1, rows, chunk), BF16),
                dma((10,)),
                dma((n_tp,)),
                dma((n_tp,)),
                dma((n_sp,)),
                dma((n_sp,)),
                dma((chunks, n_tp - 1)),
                dma((chunks, n_tp - 1)),
            ],
            compiler_params=pltpu.CompilerParams(
                collective_id=0, has_side_effects=True, vmem_limit_bytes=60 * 1024 * 1024
            ),
        )(
            tokens,
            norm_gain.reshape(1, width),
            wq,
            wk,
            wv,
            query_gain.reshape(1, hd),
            key_gain.reshape(1, hd),
            wo,
            jnp.asarray(row_np),
            jnp.asarray(col_np),
        )

    return jax.shard_map(
        per_device,
        mesh=mesh,
        in_specs=(
            P(("sp", "tp"), None),
            P(),
            P(None, "tp"),
            P(None, "tp"),
            P(None, "tp"),
            P(),
            P(),
            P("tp", None),
        ),
        out_specs=P(("sp", "tp"), None),
        check_vma=False,
    )
```

time: 136 us -> 29.3 us (0.22)
  blocking collectives: 69.3 us -> 0 us
  Pallas kernels: 0 us -> 27.7 us
  waiting for transfers between devices: 21.2 us -> 0 us
  matrix products: 17.1 us -> 0 us
  between operations: 15 us -> 0.01 us
  other arithmetic: 7.86 us -> 0 us
  local copies, waits for them, and re-layouts: 4.64 us -> 1.47 us
    all_gather x3 -> x0, blocking collectives: 69.3 us -> none  [the longest x2 62 us: folded_2(): lax.all_gather(a, axis, axis=dim, tiled=True)]
    pallas_call x0 -> x1, Pallas kernels: none -> 27.7 us  [per_device(): pl.pallas_call(functools.partial(layer_kernel, n_sp, n_tp), out_shape=jax...]
    reduce_scatter x1 -> x0, waiting for transfers between devices: 21.2 us -> none  [summed_rows(): lax.psum_scatter(everything.astype(jnp.bfloat16), axis, scatter_dimension...]
    dot_general x20 -> x0, matrix products: 17.1 us -> none  [the longest x8 9.99 us: block_scores(): jnp.einsum('kqd,skd->kqs', grouped, key_block, preferred_element_type=jnp...]
    reduce_sum x2 -> x0, other arithmetic: 2.36 us -> none  [the longest x1 1.25 us: normalize_rotate(): jnp.mean(widened * widened, axis=-1, keepdims=True) + epsilon]
    another operation x4 -> x0, other arithmetic: 1.43 us -> none
    unnamed x10 -> x1, local copies, waits for them, and re-layouts: 2.86 us -> 1.47 us
    reduce_max x2 -> x0, other arithmetic: 1.37 us -> none  [the longest x1 0.68 us: per_device(): jnp.max(jnp.abs(query_gain))]
  transfers between devices with their start and end apart: 1 -> 0, of which waited for: 1 -> 0; matrix products, arithmetic and copies ran while one was open for 0% -> 0% of each run, Pallas kernels for 0% -> 0%
where the time goes in v1:
time: 29.3 us; the launch traced here: 29.2 us
  Pallas kernels  27.7 us (95%)
  local copies, waits for them, and re-layouts  1.47 us (5%)
    pallas_call x1, Pallas kernels, per_device(): pl.pallas_call(functools.partial(layer_kernel, n_sp, n_tp), out_shape=jax...  27.7 us
    unnamed x1, local copies, waits for them, and re-layouts  1.47 us

profile of v1, /device:TPU:0, one launch (start us, length us, event | category | flops | bytes accessed | tf_op | source)
XLA Modules:
  0.0 29.2 jit_solution(17476252088958875657)
XLA Ops:
  0.0 27.7 %shard_map.100 = bf16[32,1024]{1,0:T(8,128)(2,1)} custom-call(bf16[32,1024]{1,0:T(8,128)(2,1)} %tokens.1, f32[1,1024]{1,0:T(1,128)} %bitcast.3, bf16[1024,1024]{1,0:T(8,128)(2,1)} %wq_hbm.1, bf16[1024,128]{1,0:T(8,128)(2,1)} %wk_hbm.1, bf16[1024,128]{1,0:T(8,128)(2,1)} %wv_hbm.1, f32[1,128]{1,0:T(1,128)} %bitcast.4, f32[1,128]{1,0:T(1,128)} %bitcast.5, ...), custom_call_target="tpu_custom_call" | custom-call | tf_op jit(solution)/shard_map/pallas_call | solution.py:334
  27.7 1.5 %copy.12 = bf16[32,1024]{1,0:T(8,128)(2,1)} copy(bf16[32,1024]{1,0:T(8,128)(2,1)} %shard_map.100) | data formatting | bytes 131072

commit v2 on v1

--- a/solution.py
+++ b/solution.py
@@ -50,68 +50,71 @@
         lax.fori_loop(start, stop, lambda i, c: (body(i), c)[1], 0)
 
 
-class PairExchange:
-    def __init__(self, axis, n, buf, send, recv):
-        self.axis, self.n, self.buf, self.send, self.recv = axis, n, buf, send, recv
-        self.half = n // 2
+class GroupExchange:
+    def __init__(self, axis, n, size, buf, send, recv):
+        self.axis, self.size, self.buf, self.send, self.recv = axis, size, buf, send, recv
+        self.groups = n // size
         self.me = lax.axis_index(axis)
-        self.partner = self.me + 1 - 2 * (self.me % 2)
-
-    def hop(self, i):
-        if isinstance(i, int):
-            return (i + 1) // 2 if i % 2 == 1 else self.half - i // 2
-        return (i % 2) * ((i + 1) // 2) + (1 - i % 2) * (self.half - i // 2)
-
-    def source(self, i):
-        return lax.rem(self.me + self.n - 2 * self.hop(i), self.n)
-
-    def pair_of(self, slot):
-        return slot + 1 - 2 * (slot % 2)
-
-    def copy(self, slot, sem, target):
+        self.group, self.place = self.me // size, self.me % size
+        self.parts = buf.shape[0]
+
+    def mate(self, j):
+        return self.group * self.size + lax.rem(self.place + j, self.size)
+
+    def peer(self, i):
+        return lax.rem(self.group + i, self.groups) * self.size + self.place
+
+    def source(self, i, j=0):
+        group = lax.rem(self.group + self.groups - i, self.groups)
+        return group * self.size + lax.rem(self.place + j, self.size)
+
+    def copy(self, part, slot, sem, target):
         return pltpu.make_async_remote_copy(
-            src_ref=self.buf.at[slot],
-            dst_ref=self.buf.at[slot],
-            send_sem=self.send.at[sem],
-            recv_sem=self.recv.at[slot],
+            src_ref=self.buf.at[part, slot],
+            dst_ref=self.buf.at[part, slot],
+            send_sem=self.send.at[part, sem],
+            recv_sem=self.recv.at[part, slot],
             device_id={self.axis: target},
             device_id_type=MESH,
         )
 
     def greet(self, barrier):
-        pl.semaphore_signal(barrier, inc=1, device_id={self.axis: self.partner}, device_id_type=MESH)
-
-        def one(i):
-            target = lax.rem(self.me + 2 * i, self.n)
+        def one(target):
             pl.semaphore_signal(barrier, inc=1, device_id={self.axis: target}, device_id_type=MESH)
 
-        repeat(1, self.half, one)
-        return self.half
+        repeat(1, self.groups, lambda i: one(self.peer(i)))
+        for j in range(1, self.size):
+            one(self.mate(j))
+        return self.groups + self.size - 2
 
     def start(self):
         def one(i):
-            self.copy(self.me, i, lax.rem(self.me + 2 * self.hop(i), self.n)).start()
-
-        self.copy(self.me, 0, self.partner).start()
-        repeat(1, self.half, one)
+            for part in range(self.parts):
+                self.copy(part, self.me, self.size - 2 + i, self.peer(i)).start()
+
+        repeat(1, self.groups, one)
+        for j in range(1, self.size):
+            for part in range(self.parts):
+                self.copy(part, self.me, j - 1, self.mate(j)).start()
 
     def forward(self, i):
         slot = self.source(i)
-        self.copy(slot, 0, self.partner).wait_recv()
-        self.copy(slot, self.half + i, self.partner).start()
+        first = self.groups + self.size - 2 + (i - 1) * (self.size - 1)
+        for part in range(self.parts):
+            self.copy(part, slot, 0, self.peer(i)).wait_recv()
+            for j in range(1, self.size):
+                self.copy(part, slot, first + j - 1, self.mate(j)).start()
 
     def wait_slot(self, slot):
-        self.copy(slot, 0, self.partner).wait_recv()
+        for part in range(self.parts):
+            self.copy(part, slot, 0, self.mate(1)).wait_recv()
 
     def finish(self):
         def one(i):
-            self.copy(self.me, i, self.partner).wait_send()
-
-        def two(i):
-            self.copy(self.me, self.half + i, self.partner).wait_send()
-
-        repeat(0, self.half, one)
-        repeat(1, self.half, two)
+            for part in range(self.parts):
+                self.copy(part, self.me, i, self.mate(1)).wait_send()
+
+        repeat(0, self.groups * self.size - 1, one)
 
 
 def layer_kernel(
@@ -156,15 +159,15 @@
 ):
     tp = lax.axis_index("tp")
     sp = lax.axis_index("sp")
-    rows, width = tok.shape[1], tok.shape[2]
+    rows, width = tok.shape[2], tok.shape[3]
     block = n_tp * rows
     hd = q.shape[1]
     heads = wq.shape[1] // hd
-    tokx = PairExchange("tp", n_tp, tok, tok_send, tok_recv)
-    kvx = PairExchange("sp", n_sp, kv, kv_send, kv_recv)
+    tokx = GroupExchange("tp", n_tp, 2, tok, tok_send, tok_recv)
+    kvx = GroupExchange("sp", n_sp, 4, kv, kv_send, kv_recv)
 
     local = [
-        (tokens, tok.at[tp]),
+        (tokens, tok.at[0, tp]),
         (norm_gain, gain),
         (wk_hbm, wkv.at[:, pl.ds(0, hd)]),
         (wv_hbm, wkv.at[:, pl.ds(hd, hd)]),
@@ -208,26 +211,26 @@
         return (x * cosine + swapped * sine).astype(BF16)
 
     def norm(slot):
-        x = tok[slot].astype(F32)
+        x = tok[0, slot].astype(F32)
         x = x * lax.rsqrt(jnp.mean(x * x, axis=-1, keepdims=True) + EPS) * gain[...]
         start = pl.multiple_of(slot * rows, rows)
         normed[pl.ds(start, rows), :] = x.astype(BF16)
 
     norm(tp)
-    for i in range(1, tokx.half):
+    for i in range(1, tokx.groups):
         tokx.forward(i)
-    for i in range(1, tokx.half):
         norm(tokx.source(i))
-    tokx.wait_slot(tokx.partner)
-    norm(tokx.partner)
-    for i in range(1, tokx.half):
-        slot = tokx.pair_of(tokx.source(i))
-        tokx.wait_slot(slot)
-        norm(slot)
+    for j in range(1, tokx.size):
+        tokx.wait_slot(tokx.mate(j))
+        norm(tokx.mate(j))
+    for i in range(1, tokx.groups):
+        for j in range(1, tokx.size):
+            tokx.wait_slot(tokx.source(i, j))
+            norm(tokx.source(i, j))
 
     kvp = jnp.dot(normed[...], wkv[...], preferred_element_type=F32)
-    kv[sp, 1] = kvp[:, hd:].astype(BF16)
-    kv[sp, 0] = rotate(kvp[:, :hd], kgain[...])
+    kv[1, sp] = kvp[:, hd:].astype(BF16)
+    kv[0, sp] = rotate(kvp[:, :hd], kgain[...])
     kvx.start()
 
     copies[8].wait()
@@ -242,8 +245,8 @@
 
     def fold(slot, first):
         low = slot - slot % 2
-        keys = kv[pl.ds(low, 2), 0].reshape(2 * block, hd)
-        values = kv[pl.ds(low, 2), 1].reshape(2 * block, hd)
+        keys = kv[0, pl.ds(low, 2)].reshape(2 * block, hd)
+        values = kv[1, pl.ds(low, 2)].reshape(2 * block, hd)
         for h in range(heads):
             span = slice(h * block, (h + 1) * block)
             s = lax.dot_general(
@@ -261,20 +264,22 @@
                 den[span, :] += d
                 num[span, :] += v
 
-    kvx.forward(1)
-    kvx.wait_slot(kvx.partner)
-    fold(sp, True)
-
-    def middle(i):
-        kvx.forward(i)
-        slot = kvx.source(i - 1)
-        kvx.wait_slot(kvx.pair_of(slot))
-        fold(slot, False)
-
-    repeat(2, kvx.half, middle)
-    slot = kvx.source(kvx.half - 1)
-    kvx.wait_slot(kvx.pair_of(slot))
-    fold(slot, False)
+    def fold_group(slot, first):
+        low = slot - slot % kvx.size
+        for j in range(0, kvx.size, 2):
+            fold(low + j, first and j == 0)
+
+    repeat(1, kvx.groups, kvx.forward)
+    for j in range(1, kvx.size):
+        kvx.wait_slot(kvx.mate(j))
+    fold_group(sp, True)
+
+    def other(i):
+        for j in range(1, kvx.size):
+            kvx.wait_slot(kvx.source(i, j))
+        fold_group(kvx.source(i), False)
+
+    repeat(1, kvx.groups, other)
 
     for h in range(heads):
         span = slice(h * block, (h + 1) * block)
@@ -337,7 +342,7 @@
             in_specs=[any_spec] * 10,
             out_specs=pl.BlockSpec(memory_space=pltpu.VMEM),
             scratch_shapes=[
-                vmem((n_tp, rows, width), BF16),
+                vmem((1, n_tp, rows, width), BF16),
                 vmem((1, width), F32),
                 vmem((1, hd), F32),
                 vmem((1, hd), F32),
@@ -347,7 +352,7 @@
                 vmem(row_np.shape, F32),
                 vmem(col_np.shape, F32),
                 vmem((block, width), BF16),
-                vmem((n_sp, 2, block, hd), BF16),
+                vmem((2, n_sp, block, hd), BF16),
                 vmem((heads * block, hd), BF16),
                 vmem((heads * block, hd), F32),
                 vmem((heads * block, hd), F32),
@@ -356,10 +361,10 @@
                 vmem((chunks, n_tp, rows, chunk), BF16),
                 vmem((chunks, n_tp - 1, rows, chunk), BF16),
                 dma((10,)),
-                dma((n_tp,)),
-                dma((n_tp,)),
-                dma((n_sp,)),
-                dma((n_sp,)),
+                dma((1, n_tp)),
+                dma((1, n_tp)),
+                dma((2, n_sp)),
+                dma((2, n_sp)),
                 dma((chunks, n_tp - 1)),
                 dma((chunks, n_tp - 1)),
             ],

time: 29.3 us -> 26.8 us (0.915)
  Pallas kernels: 27.7 us -> 25.2 us
    pallas_call x1, Pallas kernels: 27.7 us -> 25.2 us  [per_device(): pl.pallas_call(functools.partial(layer_kernel, n_sp, n_tp), out_shape=jax...]
where the time goes in v2:
time: 26.8 us; the launch traced here: 26.6 us
  Pallas kernels  25.2 us (94%)
  local copies, waits for them, and re-layouts  1.47 us (5%)
    pallas_call x1, Pallas kernels, per_device(): pl.pallas_call(functools.partial(layer_kernel, n_sp, n_tp), out_shape=jax...  25.2 us
    unnamed x1, local copies, waits for them, and re-layouts  1.47 us

profile of v2, /device:TPU:0, one launch (start us, length us, event | category | flops | bytes accessed | tf_op | source)
XLA Modules:
  0.0 26.6 jit_solution(17391491469215475332)
XLA Ops:
  0.0 25.2 %shard_map.100 = bf16[32,1024]{1,0:T(8,128)(2,1)} custom-call(bf16[32,1024]{1,0:T(8,128)(2,1)} %tokens.1, f32[1,1024]{1,0:T(1,128)} %bitcast.3, bf16[1024,1024]{1,0:T(8,128)(2,1)} %wq_hbm.1, bf16[1024,128]{1,0:T(8,128)(2,1)} %wk_hbm.1, bf16[1024,128]{1,0:T(8,128)(2,1)} %wv_hbm.1, f32[1,128]{1,0:T(1,128)} %bitcast.4, f32[1,128]{1,0:T(1,128)} %bitcast.5, ...), custom_call_target="tpu_custom_call" | custom-call | tf_op jit(solution)/shard_map/pallas_call | solution.py:339
  25.2 1.5 %copy.12 = bf16[32,1024]{1,0:T(8,128)(2,1)} copy(bf16[32,1024]{1,0:T(8,128)(2,1)} %shard_map.100) | data formatting | bytes 131072

commit v3 on v2

--- a/solution.py
+++ b/solution.py
@@ -163,7 +163,7 @@
     block = n_tp * rows
     hd = q.shape[1]
     heads = wq.shape[1] // hd
-    tokx = GroupExchange("tp", n_tp, 2, tok, tok_send, tok_recv)
+    tokx = GroupExchange("tp", n_tp, n_tp, tok, tok_send, tok_recv)
     kvx = GroupExchange("sp", n_sp, 4, kv, kv_send, kv_recv)
 
     local = [
@@ -330,7 +330,7 @@
         block = rows * n_tp
         heads = wq.shape[1] // hd
         out_width = wo.shape[1]
-        chunks = 4
+        chunks = 2
         chunk = out_width // chunks
         row_np, col_np = angle_tables(block * n_sp // GRID_W, hd)
         vmem = pltpu.VMEM

time: 26.8 us -> 26.4 us (0.985)
  Pallas kernels: 25.2 us -> 24.7 us
    pallas_call x1, Pallas kernels: 25.2 us -> 24.7 us  [per_device(): pl.pallas_call(functools.partial(layer_kernel, n_sp, n_tp), out_shape=jax...]
where the time goes in v3:
time: 26.4 us; the launch traced here: 26.2 us
  Pallas kernels  24.7 us (94%)
  local copies, waits for them, and re-layouts  1.47 us (6%)
    pallas_call x1, Pallas kernels, per_device(): pl.pallas_call(functools.partial(layer_kernel, n_sp, n_tp), out_shape=jax...  24.7 us
    unnamed x1, local copies, waits for them, and re-layouts  1.47 us

profile of v3, /device:TPU:0, one launch (start us, length us, event | category | flops | bytes accessed | tf_op | source)
XLA Modules:
  0.0 26.2 jit_solution(14923329594879188962)
XLA Ops:
  0.0 24.7 %shard_map.100 = bf16[32,1024]{1,0:T(8,128)(2,1)} custom-call(bf16[32,1024]{1,0:T(8,128)(2,1)} %tokens.1, f32[1,1024]{1,0:T(1,128)} %bitcast.3, bf16[1024,1024]{1,0:T(8,128)(2,1)} %wq_hbm.1, bf16[1024,128]{1,0:T(8,128)(2,1)} %wk_hbm.1, bf16[1024,128]{1,0:T(8,128)(2,1)} %wv_hbm.1, f32[1,128]{1,0:T(1,128)} %bitcast.4, f32[1,128]{1,0:T(1,128)} %bitcast.5, ...), custom_call_target="tpu_custom_call" | custom-call | tf_op jit(solution)/shard_map/pallas_call | solution.py:339
  24.7 1.5 %copy.12 = bf16[32,1024]{1,0:T(8,128)(2,1)} copy(bf16[32,1024]{1,0:T(8,128)(2,1)} %shard_map.100) | data formatting | bytes 131072
